TPU v7x, 32 devices: a whole 2x2x4 slice. The times are simulated.
32 devices in a mesh: tp: 8 (over z, x), dp: 4 (over y, core).
Axes of the slice: x: 2, y: 2, z: 4, core: 2. Of those that a mesh axis runs over, the one named last changes fastest.
Arguments:
- tokens: bfloat16 [128, 8, 4096], P('dp', None, 'tp'), may hold values from -12 to 12
- lengths: int32 [128], P('dp'), may hold values from 1 to 8, 384 in all
- norm_gains: float32 [2, 4096], replicated, may hold values from 0.1 to 1.9
- drive_proj: bfloat16 [2, 4096, 2048], P(None, 'dp', 'tp'), may hold values from -0.09375 to 0.09375
- open_proj: bfloat16 [2, 4096, 4096], P(None, 'dp', 'tp'), may hold values from -0.09375 to 0.09375
- glu_proj: bfloat16 [2, 2048, 2048], P(None, 'dp', 'tp'), may hold values from -0.125 to 0.125
- merge_proj: bfloat16 [2, 2048, 4096], P(None, 'dp', 'tp'), may hold values from -0.125 to 0.125
- exit_proj: bfloat16 [2, 4096, 4096], P(None, 'dp', 'tp'), may hold values from -0.09375 to 0.09375
- decay_rate: float32 [2, 128, 64], P(None, 'tp'), may hold values from 0.5 to 2
- turn_rate: float32 [2, 128, 64], P(None, 'tp'), may hold values from -3 to 3
- group_step_width: float32 [2, 128], P(None, 'tp'), may hold values from 0.005 to 0.3
- state_in: float32 [2, 2, 128, 64, 16], P(None, None, 'tp'), may hold values from -1 to 1
- state_out: float32 [2, 2, 128, 16, 64], P(None, None, 'tp'), may hold values from -0.5 to 0.5
- skip_gain: float32 [2, 2048], P(None, 'tp'), may hold values from -4 to 4
- carried_state: float32 [2, 2, 128, 8192], P(None, None, 'dp', 'tp'), may hold values from -6 to 6
Outputs:
- updated_tokens: bfloat16 [128, 8, 4096], P('dp', None, 'tp')
- new_state: float32 [2, 2, 128, 8192], P(None, None, 'dp', 'tp')
Inputs may be any that keep to these rules, and one draw needn't show every extreme that they name: `lengths`: each sequence has at least one live slot, and some sequence has all 8.
All inputs are finite; a program needn't handle non-finite values. No bound on the sum of `lengths` on one device may be relied on, other than what follows from the above.
Results may differ from a plain program's by a relative error of at most 0.0055.
Values may be sent and summed in bfloat16 or wider, within the bound.
A program may use at most 128 MiB of HBM per device.

v0:
```python
import jax
import jax.numpy as jnp
from jax import lax
from jax.sharding import PartitionSpec as P

EPS = 1e-05


def state_update(
    drive, active, current_rate, turn_now, size_now, in_pair, output_couple, skip_now, carried
):
    sequences, positions = active.shape
    groups, entries = current_rate.shape
    members = in_pair.shape[-1]
    real_eig = -current_rate
    step_len = size_now[:, None]
    magnitude = jnp.exp(step_len * real_eig)
    decay_real = magnitude * jnp.cos(step_len * turn_now)
    decay_imag = magnitude * jnp.sin(step_len * turn_now)
    divisor = real_eig * real_eig + turn_now * turn_now
    hold_real = ((decay_real - 1.0) * real_eig + decay_imag * turn_now) / divisor
    hold_imag = (decay_imag * real_eig - (decay_real - 1.0) * turn_now) / divisor
    inject_real = hold_real[..., None] * in_pair[0] - hold_imag[..., None] * in_pair[1]
    inject_imag = hold_real[..., None] * in_pair[1] + hold_imag[..., None] * in_pair[0]
    inputs = drive.reshape(sequences, positions, groups, members)
    pushed_real = jnp.einsum("gpc,bsgc->bsgp", inject_real, inputs, precision=lax.Precision.HIGHEST)
    pushed_imag = jnp.einsum("gpc,bsgc->bsgp", inject_imag, inputs, precision=lax.Precision.HIGHEST)
    state_real_part = carried[0].reshape(sequences, groups, entries)
    state_imaginary = carried[1].reshape(sequences, groups, entries)
    readings = []
    for position in range(positions):
        active_now = (active[:, position] > 0)[:, None, None]
        moved_real = (
            decay_real * state_real_part - decay_imag * state_imaginary + pushed_real[:, position]
        )
        moved_imag = (
            decay_real * state_imaginary + decay_imag * state_real_part + pushed_imag[:, position]
        )
        state_real_part = jnp.where(active_now, moved_real, state_real_part)
        state_imaginary = jnp.where(active_now, moved_imag, state_imaginary)
        readout_value = jnp.einsum(
            "sal,usl->usa", output_couple[0], state_real_part, precision=lax.Precision.HIGHEST
        ) - jnp.einsum(
            "sal,usl->usa", output_couple[1], state_imaginary, precision=lax.Precision.HIGHEST
        )
        readings.append(readout_value)
    readout = jnp.stack(readings, axis=1) + skip_now.reshape(groups, members) * inputs
    final = jnp.stack(
        [
            state_real_part.reshape(sequences, groups * entries),
            state_imaginary.reshape(sequences, groups * entries),
        ]
    )
    return (readout.reshape(sequences * positions, groups * members), final)


def widen_model(values):
    return lax.all_gather(values, "tp", axis=1, tiled=True)


def widen_branch(values):
    return lax.all_gather(values, "tp", axis=1, tiled=True)


def project(gathered, weight):
    return jnp.dot(
        gathered,
        lax.all_gather(weight, "dp", axis=0, tiled=True),
        preferred_element_type=jnp.float32,
    )


def shards(
    tokens,
    lengths,
    norm_gains,
    drive_proj,
    open_proj,
    glu_proj,
    merge_proj,
    exit_proj,
    decay_rate,
    turn_rate,
    group_step_width,
    state_in,
    state_out,
    skip_gain,
    carried_state,
):
    sequences, positions, local_width = tokens.shape
    row_count = sequences * positions
    model_width = local_width * lax.axis_size("tp")
    first_col = lax.axis_index("tp") * local_width
    active = (lax.broadcasted_iota(jnp.int32, (sequences, positions), 1) < lengths[:, None]).astype(
        jnp.int32
    )
    active_rows = active.reshape(row_count, 1).astype(jnp.float32)
    residual = tokens.reshape(row_count, local_width)
    states = []
    for layer_index in range(norm_gains.shape[0]):
        norm_gain = norm_gains[layer_index]
        own_values = residual.astype(jnp.float32)
        squared_sum = lax.psum(jnp.sum(own_values * own_values, axis=1), "tp")
        inverse_rms = lax.rsqrt(squared_sum / model_width + EPS)[:, None]
        own_gain = lax.dynamic_slice_in_dim(norm_gain, first_col, local_width, 0)
        gathered = widen_model((own_values * inverse_rms * own_gain).astype(jnp.bfloat16))
        drive = project(gathered, drive_proj[layer_index])
        gate_open = jax.nn.sigmoid(project(gathered, open_proj[layer_index]))
        readout, final = state_update(
            drive,
            active,
            decay_rate[layer_index],
            turn_rate[layer_index],
            group_step_width[layer_index],
            state_in[layer_index],
            state_out[layer_index],
            skip_gain[layer_index],
            carried_state[layer_index],
        )
        states.append(final)
        activated = jax.nn.gelu(readout).astype(jnp.bfloat16)
        gating = project(widen_branch(activated), glu_proj[layer_index])
        gated = (activated.astype(jnp.float32) * jax.nn.sigmoid(gating)).astype(jnp.bfloat16)
        merged = project(widen_branch(gated), merge_proj[layer_index])
        mixed = (gate_open * merged).astype(jnp.bfloat16)
        branch = project(widen_model(mixed), exit_proj[layer_index])
        residual = (residual.astype(jnp.float32) + active_rows * branch).astype(jnp.bfloat16)
    return (residual.reshape(sequences, positions, local_width), jnp.stack(states))


def solution(mesh):
    in_specs = (
        P("dp", None, "tp"),
        P("dp"),
        P(),
        P(None, "dp", "tp"),
        P(None, "dp", "tp"),
        P(None, "dp", "tp"),
        P(None, "dp", "tp"),
        P(None, "dp", "tp"),
        P(None, "tp", None),
        P(None, "tp", None),
        P(None, "tp"),
        P(None, None, "tp", None, None),
        P(None, None, "tp", None, None),
        P(None, "tp"),
        P(None, None, "dp", "tp"),
    )
    out_specs = (P("dp", None, "tp"), P(None, None, "dp", "tp"))
    return jax.shard_map(shards, mesh=mesh, in_specs=in_specs, out_specs=out_specs, check_vma=False)
```

profile of v0, /device:TPU:0, one launch (start us, length us, event | category | flops | bytes accessed | tf_op | source)
XLA Modules:
  0.0 707.5 jit_solution(4428971721815651498)
XLA Ops:
  9.9 23.1 %psum.14 = f32[256]{0:T(256)S(1)} all-reduce(f32[256]{0:T(256)S(1)} %reduce_sum.21), channel_id=1, replica_groups=mesh['tp'=8,'dp'=4] {'tp'}, use_global_device_ids=true, to_apply=%region_1.0 | all-reduce | flops 256 | bytes 2048 | tf_op jit(solution)/shard_map/psum | solution.py:103
  41.2 47.3 %all-gather.29.cloned.1.call-done = bf16[256,4096]{1,0:T(8,128)(2,1)} async-done(((bf16[256,512]{1,0:T(8,128)(2,1)}), bf16[256,4096]{1,0:T(8,128)(2,1)}) %all-gather.29.cloned.1.call-update) | async-done | bytes 2097168 | tf_op jit(solution)/shard_map/all_gather | solution.py:58
  93.4 4.9 fusion.23
  117.4 4.0 copy.50
  131.7 32.2 %all-gather.31.cloned.1.call-done = bf16[256,2048]{1,0:T(8,128)(2,1)} async-done(((bf16[256,256]{1,0:T(8,128)(2,1)}), bf16[256,2048]{1,0:T(8,128)(2,1)}) %all-gather.31.cloned.1.call-update) | async-done | bytes 1048592 | tf_op jit(solution)/shard_map/all_gather | solution.py:62
  169.6 29.1 %all-gather.45.cloned.1.call-done = bf16[1,4096,512]{2,1,0:T(8,128)(2,1)} async-done(((bf16[1,1024,512]{2,1,0:T(8,128)(2,1)}), bf16[1,4096,512]{2,1,0:T(8,128)(2,1)}) %all-gather.45.cloned.1.call-update) | async-done | bytes 4194320 | tf_op jit(solution)/shard_map/all_gather | solution.py:68
  198.8 4.9 fusion.59
  203.7 19.1 %all-gather.51.cloned.1.call-done = bf16[1,2048,512]{2,1,0:T(8,128)(2,1)} async-done(((bf16[1,512,512]{2,1,0:T(8,128)(2,1)}), bf16[1,2048,512]{2,1,0:T(8,128)(2,1)}) %all-gather.51.cloned.1.call-update) | async-done | bytes 2097168 | tf_op jit(solution)/shard_map/all_gather | solution.py:68
  222.8 42.0 %all-gather.33.cloned.1.call-done = bf16[256,2048]{1,0:T(8,128)(2,1)} async-done(((bf16[256,256]{1,0:T(8,128)(2,1)}), bf16[256,2048]{1,0:T(8,128)(2,1)}) %all-gather.33.cloned.1.call-update) | async-done | bytes 1048592 | tf_op jit(solution)/shard_map/all_gather | solution.py:62
  272.9 27.0 %all-gather.53.cloned.1.call-done = bf16[1,4096,512]{2,1,0:T(8,128)(2,1)} async-done(((bf16[1,1024,512]{2,1,0:T(8,128)(2,1)}), bf16[1,4096,512]{2,1,0:T(8,128)(2,1)}) %all-gather.53.cloned.1.call-update) | async-done | bytes 4194320 | tf_op jit(solution)/shard_map/all_gather | solution.py:68
  299.9 53.0 %all-gather.35.cloned.1.call-done = bf16[256,4096]{1,0:T(8,128)(2,1)} async-done(((bf16[256,512]{1,0:T(8,128)(2,1)}), bf16[256,4096]{1,0:T(8,128)(2,1)}) %all-gather.35.cloned.1.call-update) | async-done | bytes 2097168 | tf_op jit(solution)/shard_map/all_gather | solution.py:58
  352.9 5.5 multiply_reduce_fusion
  358.4 18.7 %psum.15 = f32[256]{0:T(256)S(1)} all-reduce(f32[256]{0:T(256)} %get-tuple-element.117), channel_id=1, replica_groups=mesh['tp'=8,'dp'=4] {'tp'}, use_global_device_ids=true, to_apply=%region_3.4 | all-reduce | flops 256 | bytes 2048 | tf_op jit(solution)/shard_map/psum | solution.py:103
  382.5 45.6 %all-gather.37.cloned.1.call-done = bf16[256,4096]{1,0:T(8,128)(2,1)} async-done(((bf16[256,512]{1,0:T(8,128)(2,1)}), bf16[256,4096]{1,0:T(8,128)(2,1)}) %all-gather.37.cloned.1.call-update) | async-done | bytes 2097168 | tf_op jit(solution)/shard_map/all_gather | solution.py:58
  436.6 4.9 convolution_bitcast_fusion
  441.6 5.3 convolution_bitcast_fusion.1
  462.0 4.0 copy.61
  470.5 36.6 %all-gather.39.cloned.1.call-done = bf16[256,2048]{1,0:T(8,128)(2,1)} async-done(((bf16[256,256]{1,0:T(8,128)(2,1)}), bf16[256,2048]{1,0:T(8,128)(2,1)}) %all-gather.39.cloned.1.call-update) | async-done | bytes 1048592 | tf_op jit(solution)/shard_map/all_gather | solution.py:62
  510.4 31.6 %all-gather.55.cloned.1.call-done = bf16[1,4096,512]{2,1,0:T(8,128)(2,1)} async-done(((bf16[1,1024,512]{2,1,0:T(8,128)(2,1)}), bf16[1,4096,512]{2,1,0:T(8,128)(2,1)}) %all-gather.55.cloned.1.call-update) | async-done | bytes 4194320 | tf_op jit(solution)/shard_map/all_gather | solution.py:68
  542.0 4.1 fusion.53
  546.1 19.9 %all-gather.61.cloned.1.call-done = bf16[1,2048,512]{2,1,0:T(8,128)(2,1)} async-done(((bf16[1,512,512]{2,1,0:T(8,128)(2,1)}), bf16[1,2048,512]{2,1,0:T(8,128)(2,1)}) %all-gather.61.cloned.1.call-update) | async-done | bytes 2097168 | tf_op jit(solution)/shard_map/all_gather | solution.py:68
  566.0 41.9 %all-gather.41.cloned.1.call-done = bf16[256,2048]{1,0:T(8,128)(2,1)} async-done(((bf16[256,256]{1,0:T(8,128)(2,1)}), bf16[256,2048]{1,0:T(8,128)(2,1)}) %all-gather.41.cloned.1.call-update) | async-done | bytes 1048592 | tf_op jit(solution)/shard_map/all_gather | solution.py:62
  655.5 40.2 %all-gather.43.cloned.1.call-done = bf16[256,4096]{1,0:T(8,128)(2,1)} async-done(((bf16[256,512]{1,0:T(8,128)(2,1)}), bf16[256,4096]{1,0:T(8,128)(2,1)}) %all-gather.43.cloned.1.call-update) | async-done | bytes 2097168 | tf_op jit(solution)/shard_map/all_gather | solution.py:58
  695.7 4.8 fusion.83
  (378 shorter events, 142.0 us)
Async XLA Ops:
  7.2 33.9 %all-gather.47.cloned.1.call-start = ((), (), s32[]{:S(2)}) async-start(), calls=%async_computation.9 | async-start | bytes 2621440 | tf_op jit(solution)/shard_map/all_gather | solution.py:68
  9.6 28.7 %copy-start.7 = (f32[2,2,32,1024]{3,2,1,0:T(8,128)S(1)}, f32[2,2,32,1024]{3,2,1,0:T(8,128)}, u32[]{:S(2)}) copy-start(f32[2,2,32,1024]{3,2,1,0:T(8,128)} %param.29) | copy-start | bytes 1572868
  9.6 78.9 %all-gather.29.cloned.1.call-start = ((), (), s32[]{:S(2)}) async-start(), calls=%async_computation | async-start | bytes 2359296 | tf_op jit(solution)/shard_map/all_gather | solution.py:58
  9.9 30.7 %copy-start.86 = (f32[2,256]{1,0:T(2,128)S(1)}, f32[2,256]{1,0:T(2,128)}, u32[]{:S(2)}) copy-start(f32[2,256]{1,0:T(2,128)} %param.28) | copy-start | bytes 6148
  34.5 97.2 %all-gather.49.cloned.1.call-start = ((), (), s32[]{:S(2)}) async-start(), calls=%async_computation.10 | async-start | bytes 1310720 | tf_op jit(solution)/shard_map/all_gather | solution.py:68
  35.5 128.4 %all-gather.31.cloned.1.call-start = ((), (), s32[]{:S(2)}) async-start(), calls=%async_computation.1 | async-start | bytes 1179648 | tf_op jit(solution)/shard_map/all_gather | solution.py:62
  126.2 72.6 %all-gather.45.cloned.1.call-start = ((), (), s32[]{:S(2)}) async-start(), calls=%async_computation.8 | async-start | bytes 5242880 | tf_op jit(solution)/shard_map/all_gather | solution.py:68
  129.2 34.7 %copy-start.43 = (bf16[256,256]{1,0:T(8,128)(2,1)S(1)}, bf16[256,256]{1,0:T(8,128)(2,1)}, u32[]{:S(2)}) copy-start(bf16[256,256]{1,0:T(8,128)(2,1)} %fusion.141) | copy-start | bytes 393220
  129.2 93.6 %all-gather.51.cloned.1.call-start = ((), (), s32[]{:S(2)}) async-start(), calls=%async_computation.11 | async-start | bytes 2621440 | tf_op jit(solution)/shard_map/all_gather | solution.py:68
  131.6 133.2 %all-gather.33.cloned.1.call-start = ((), (), s32[]{:S(2)}) async-start(), calls=%async_computation.2 | async-start | bytes 1179648 | tf_op jit(solution)/shard_map/all_gather | solution.py:62
  166.5 133.4 %all-gather.53.cloned.1.call-start = ((), (), s32[]{:S(2)}) async-start(), calls=%async_computation.12 | async-start | bytes 5242880 | tf_op jit(solution)/shard_map/all_gather | solution.py:68
  169.6 183.3 %all-gather.35.cloned.1.call-start = ((), (), s32[]{:S(2)}) async-start(), calls=%async_computation.3 | async-start | bytes 2359296 | tf_op jit(solution)/shard_map/all_gather | solution.py:58
  203.7 149.2 %copy-start.33 = (bf16[32,8,512]{2,1,0:T(8,128)(2,1)S(1)}, bf16[32,8,512]{2,1,0:T(8,128)(2,1)}, u32[]{:S(2)}) copy-start(bf16[32,8,512]{2,1,0:T(8,128)(2,1)} %param.15) | copy-start | bytes 786436
  268.2 114.3 %all-gather.57.cloned.1.call-start = ((), (), s32[]{:S(2)}) async-start(), calls=%async_computation.14 | async-start | bytes 2621440 | tf_op jit(solution)/shard_map/all_gather | solution.py:68
  268.8 159.3 %all-gather.37.cloned.1.call-start = ((), (), s32[]{:S(2)}) async-start(), calls=%async_computation.4 | async-start | bytes 2359296 | tf_op jit(solution)/shard_map/all_gather | solution.py:58
  379.0 91.5 %all-gather.59.cloned.1.call-start = ((), (), s32[]{:S(2)}) async-start(), calls=%async_computation.15 | async-start | bytes 1310720 | tf_op jit(solution)/shard_map/all_gather | solution.py:68
  379.6 127.5 %all-gather.39.cloned.1.call-start = ((), (), s32[]{:S(2)}) async-start(), calls=%async_computation.5 | async-start | bytes 1179648 | tf_op jit(solution)/shard_map/all_gather | solution.py:62
  469.3 72.7 %all-gather.55.cloned.1.call-start = ((), (), s32[]{:S(2)}) async-start(), calls=%async_computation.13 | async-start | bytes 5242880 | tf_op jit(solution)/shard_map/all_gather | solution.py:68
  469.8 96.2 %all-gather.61.cloned.1.call-start = ((), (), s32[]{:S(2)}) async-start(), calls=%async_computation.16 | async-start | bytes 2621440 | tf_op jit(solution)/shard_map/all_gather | solution.py:68
  470.4 137.5 %all-gather.41.cloned.1.call-start = ((), (), s32[]{:S(2)}) async-start(), calls=%async_computation.6 | async-start | bytes 1179648 | tf_op jit(solution)/shard_map/all_gather | solution.py:62
  509.7 145.7 %all-gather.63.cloned.1.call-start = ((), (), s32[]{:S(2)}) async-start(), calls=%async_computation.17 | async-start | bytes 5242880 | tf_op jit(solution)/shard_map/all_gather | solution.py:68
  510.3 185.4 %all-gather.43.cloned.1.call-start = ((), (), s32[]{:S(2)}) async-start(), calls=%async_computation.7 | async-start | bytes 2359296 | tf_op jit(solution)/shard_map/all_gather | solution.py:58
  654.3 41.4 %copy-start.44 = (f32[256,512]{1,0:T(8,128)S(1)}, f32[256,512]{1,0:T(8,128)}, u32[]{:S(2)}) copy-start(f32[256,512]{1,0:T(8,128)} %get-tuple-element.118) | copy-start | bytes 1572868
  654.3 41.4 %copy-start.87 = (f32[256]{0:T(256)S(1)}, f32[256]{0:T(256)}, u32[]{:S(2)}) copy-start(f32[256]{0:T(256)} %convert_element_type.74) | copy-start | bytes 3076
  (84 other events, 496.4 us)
Sparse Core Ops, SparseCore 0:
  10.2 25.2 all-gather.46
  38.1 50.3 all-gather.28
  90.1 14.8 all-gather.48
  126.3 37.5 all-gather.30
  165.3 33.4 all-gather.44
  200.2 22.5 all-gather.50
  225.4 39.3 all-gather.32
  266.4 33.4 all-gather.52
  302.5 50.3 all-gather.34
  354.3 20.7 all-gather.56
  379.1 48.9 all-gather.36
  429.5 14.8 all-gather.58
  469.4 37.6 all-gather.38
  508.5 33.4 all-gather.54
  543.4 22.5 all-gather.60
  568.5 39.3 all-gather.40
  609.3 33.4 all-gather.62
  645.3 50.3 all-gather.42
where the time goes:
time: 718 us; the launch traced here: 708 us
  waiting for transfers between devices  468 us (65%)
  matrix products  83.7 us (12%)
  local copies, waits for them, and re-layouts  80.9 us (11%)
  blocking collectives  41.8 us (6%)
  other arithmetic  15.8 us (2%)
  between operations  15.8 us (2%)
    all_gather x4, waiting for transfers between devices, widen_model(): return lax.all_gather(values, 'tp', axis=1, tiled=True)  186 us
    all_gather x4, waiting for transfers between devices, widen_branch(): return lax.all_gather(values, 'tp', axis=1, tiled=True)  153 us
    all_gather x10, waiting for transfers between devices, project(): lax.all_gather(weight, 'dp', axis=0, tiled=True)  127 us
    psum x2, blocking collectives, shards(): squared_sum = lax.psum(jnp.sum(own_values * own_values, axis=1), 'tp')  41.8 us
    dot_general x10, matrix products, project(): jnp.dot(gathered, lax.all_gather(weight, 'dp', axis=0, tiled=True), prefe...  37.3 us
    dot_general x16, matrix products, state_update(): jnp.einsum('sal,usl->usa', output_couple[1], state_imaginary, precision=l...  19.5 us
  transfers between devices with their start and end apart: 18, of which 13 were waited for; matrix products, arithmetic and copies ran while one was open for 24% of the time, Pallas kernels for 0%

commit v1 on v0

--- a/solution.py
+++ b/solution.py
@@ -1,6 +1,9 @@
+import functools
 import jax
 import jax.numpy as jnp
 from jax import lax
+from jax.experimental import pallas as pl
+from jax.experimental.pallas import tpu as pltpu
 from jax.sharding import PartitionSpec as P
 
 EPS = 1e-05
@@ -128,6 +131,399 @@
     return (residual.reshape(sequences, positions, local_width), jnp.stack(states))
 
 
+def fused_kernel(
+    dims,
+    tok, pack_own, unpack_own, keep, unpack, pack, gains, decay, inject, outmix, skip, carried,
+    w_drive, w_open, w_glu, w_merge, w_exit,
+    out_tok, out_state,
+    v_drive, v_open, v_glu, v_merge, v_exit,
+    row_send, row_recv, a_send, a_recv, c_send, c_recv,
+    x_src, x_recv, y_src, y_recv, st_recv, st_new, nst_recv, fin_recv,
+    inv_buf, gate_buf, act_buf,
+    w_sem, row_ss, row_rs, a_ss, a_rs, c_ss, c_rs, x_ss, x_rs, y_ss, y_rs,
+    st_ss, st_rs, n_ss, n_rs, f_ss, f_rs,
+):
+    layers, nd, nt, rows, model = dims
+    ratio = nt // nd
+    chunk = rows // nd
+    half = rows // 2
+    f32, bf16 = jnp.float32, jnp.bfloat16
+    d = lax.axis_index("dp")
+    t = lax.axis_index("tp")
+    home = t // ratio
+    place = lax.rem(t, ratio)
+    batch_own = carried.shape[2]
+    batch = batch_own * nd
+    own_ch = inject.shape[2] // 2
+    width = c_send.shape[-1] // 2
+    steps = unpack.shape[0] // batch
+
+    loads = []
+    for i, (src, dst) in enumerate(
+        ((w_drive, v_drive), (w_open, v_open), (w_glu, v_glu), (w_merge, v_merge), (w_exit, v_exit))
+    ):
+        for l in range(layers):
+            copy = pltpu.make_async_copy(src.at[l], dst.at[l], w_sem.at[i, l])
+            copy.start()
+            loads.append(copy)
+
+    def weight(i, l):
+        loads[i * layers + l].wait()
+
+    barrier = pltpu.get_barrier_semaphore()
+    total = nd * nt
+    flat = t * nd + d
+
+    def greet(i, carry):
+        other = lax.rem(flat + i, total)
+        pl.semaphore_signal(
+            barrier, inc=1,
+            device_id={"tp": other // nd, "dp": lax.rem(other, nd)},
+            device_id_type=pl.DeviceIdType.MESH,
+        )
+        return carry
+
+    lax.fori_loop(1, total, greet, 0)
+    pl.semaphore_wait(barrier, total - 1)
+
+    pending = []
+
+    def send(src, dst, ss, rs, to_dp, to_tp, is_self):
+        far = pltpu.make_async_remote_copy(
+            src_ref=src, dst_ref=dst, send_sem=ss, recv_sem=rs,
+            device_id={"tp": to_tp, "dp": to_dp}, device_id_type=pl.DeviceIdType.MESH,
+        )
+        if is_self is None:
+            far.start()
+        else:
+            @pl.when(is_self)
+            def _():
+                pltpu.make_async_copy(src, dst, rs).start()
+
+            @pl.when(jnp.logical_not(is_self))
+            def _():
+                far.start()
+
+        pending.append((far, is_self))
+
+    def arrive(dst, rs):
+        pltpu.make_async_copy(dst, dst, rs).wait()
+
+    def send_row(k, c):
+        send(row_send.at[k, c], row_recv.at[k, d], row_ss.at[k, c], row_rs.at[k, d], c, t, d == c)
+
+    def row_sum(k):
+        acc = None
+        for s in range(nd):
+            arrive(row_recv.at[k, s], row_rs.at[k, s])
+            v = row_recv[k, s].astype(f32)
+            acc = v if acc is None else acc + v
+        return acc
+
+    def spread_x(k):
+        slot = place * nd + d
+        for j in range(nt):
+            to = lax.rem(t + j, nt)
+            send(
+                x_src.at[k], x_recv.at[k, place, pl.ds(d * chunk, chunk)],
+                x_ss.at[k, j], x_rs.at[k, slot], home, to, (d == home) if j == 0 else None,
+            )
+
+    def take_x(k):
+        for p in range(ratio):
+            for s in range(nd):
+                arrive(x_recv.at[k, p, pl.ds(s * chunk, chunk)], x_rs.at[k, p * nd + s])
+
+    def spread_y(k):
+        slot = place * nd + d
+        for j in range(nt):
+            to = lax.rem(t + j, nt)
+            send(
+                y_src.at[k], y_recv.at[k, slot],
+                y_ss.at[k, j], y_rs.at[k, slot], home, to, (d == home) if j == 0 else None,
+            )
+
+    def take_y(k):
+        parts = []
+        for p in range(ratio):
+            for s in range(nd):
+                arrive(y_recv.at[k, p * nd + s], y_rs.at[k, p * nd + s])
+                v = y_recv[k, p * nd + s]
+                parts.append(jnp.concatenate([v[:, :width], v[:, width:]], axis=0))
+        return jnp.concatenate(parts, axis=1)
+
+    def fold(v):
+        return jnp.concatenate([v[:half], v[half:]], axis=1)
+
+    for c in range(nd):
+        part = jnp.dot(pack_own[c * chunk:(c + 1) * chunk, :], tok[...], preferred_element_type=f32)
+        row_send[0, c] = part.astype(bf16)
+        send_row(0, c)
+    for c in range(nd):
+        send(
+            carried.at[:, :, :, pl.ds(c * own_ch, own_ch)], st_recv.at[d],
+            st_ss.at[c], st_rs.at[d], c, t, d == c,
+        )
+    residual = row_sum(0).astype(bf16)
+    cols = tok.shape[1]
+    for l in range(layers):
+        x_src[2 * l] = residual
+        spread_x(2 * l)
+        if l == 0:
+            for s in range(nd):
+                arrive(st_recv.at[s], st_rs.at[s])
+        take_x(2 * l)
+        scaled, squares = [], None
+        for p in range(ratio):
+            raw = x_recv[2 * l, p].astype(f32)
+            sq = jnp.sum(raw * raw, axis=1, keepdims=True)
+            squares = sq if squares is None else squares + sq
+            scaled.append((raw * gains[l, p]).astype(bf16))
+        normed = jnp.concatenate(scaled, axis=1)
+        weight(0, l)
+        drive = jnp.dot(normed, v_drive[l], preferred_element_type=f32)
+        high = squares.astype(bf16)
+        low = (squares - high.astype(f32)).astype(bf16)
+        lane = lax.broadcasted_iota(jnp.int32, (rows, width), 1)
+        tail = jnp.where(
+            lane == 0, high.astype(f32), jnp.where(lane == 1, low.astype(f32), 0.0)
+        ).astype(bf16)
+        for c in range(nd):
+            a_send[l, c] = jnp.concatenate(
+                [drive[:, c * width:(c + 1) * width].astype(bf16), tail], axis=1
+            )
+            send(a_send.at[l, c], a_recv.at[l, d], a_ss.at[l, c], a_rs.at[l, d], c, t, d == c)
+        weight(1, l)
+        k_open = 1 + 3 * l
+        for c in range(nd):
+            part = jnp.dot(
+                normed[c * chunk:(c + 1) * chunk], v_open[l], preferred_element_type=f32
+            )
+            row_send[k_open, c] = part.astype(bf16)
+            send_row(k_open, c)
+        summed = None
+        for s in range(nd):
+            arrive(a_recv.at[l, s], a_rs.at[l, s])
+            v = a_recv[l, s].astype(f32)
+            summed = v if summed is None else summed + v
+        full_sq = summed[:, width:width + 1] + summed[:, width + 1:width + 2]
+        inverse = lax.rsqrt(full_sq / model + EPS)
+        inv_buf[...] = jnp.broadcast_to(inverse, inv_buf.shape)
+        lane2 = lax.broadcasted_iota(jnp.int32, summed.shape, 1)
+        feed = jnp.where(lane2 < width, summed * inverse, jnp.where(lane2 == width, 1.0, 0.0))
+        feed = feed.astype(bf16)
+        real = jnp.concatenate([st_recv[s, l, 0] for s in range(nd)], axis=0)
+        imag = jnp.concatenate([st_recv[s, l, 1] for s in range(nd)], axis=0)
+        dr, di = decay[l, 0], decay[l, 1]
+        for step in range(steps):
+            span = slice(step * batch, (step + 1) * batch)
+            u = jnp.dot(unpack[span, :], feed, preferred_element_type=f32)
+            live = u[:, width:width + 1] > 0.5
+            push = jnp.dot(u.astype(bf16), inject[l], preferred_element_type=f32)
+            moved_real = dr * real - di * imag + push[:, :own_ch]
+            moved_imag = dr * imag + di * real + push[:, own_ch:]
+            real = jnp.where(live, moved_real, real)
+            imag = jnp.where(live, moved_imag, imag)
+            both = jnp.concatenate([real, imag], axis=1).astype(bf16)
+            read = jnp.dot(both, outmix[l], preferred_element_type=f32) + skip[l] * u
+            act_buf[span, :] = jax.nn.gelu(read).astype(bf16)
+        st_new[l, 0] = real
+        st_new[l, 1] = imag
+        packed = jnp.dot(pack[...], act_buf[...], preferred_element_type=f32).astype(bf16)
+        activated = fold(packed[:, :width])
+        y_src[2 * l] = activated
+        spread_y(2 * l)
+        for c in range(nd):
+            send(
+                st_new.at[l, :, pl.ds(c * batch_own, batch_own)], nst_recv.at[d, l],
+                n_ss.at[l, c], n_rs.at[l, d], c, t, d == c,
+            )
+        mine = pl.ds(pl.multiple_of(d * chunk, chunk), chunk)
+        gate_buf[...] = jax.nn.sigmoid(row_sum(k_open) * inv_buf[mine, 0:1])
+        wide = take_y(2 * l)
+        weight(2, l)
+        gating = jnp.dot(wide, v_glu[l], preferred_element_type=f32).astype(bf16)
+        for c in range(nd):
+            c_send[l, c] = fold(gating[:, c * width:(c + 1) * width])
+            send(c_send.at[l, c], c_recv.at[l, d], c_ss.at[l, c], c_rs.at[l, d], c, t, d == c)
+        summed = None
+        for s in range(nd):
+            arrive(c_recv.at[l, s], c_rs.at[l, s])
+            v = c_recv[l, s].astype(f32)
+            summed = v if summed is None else summed + v
+        y_src[2 * l + 1] = (activated.astype(f32) * jax.nn.sigmoid(summed)).astype(bf16)
+        spread_y(2 * l + 1)
+        wide = take_y(2 * l + 1)
+        weight(3, l)
+        for c in range(nd):
+            part = jnp.dot(wide[c * chunk:(c + 1) * chunk], v_merge[l], preferred_element_type=f32)
+            row_send[k_open + 1, c] = part.astype(bf16)
+            send_row(k_open + 1, c)
+        x_src[2 * l + 1] = (gate_buf[...] * row_sum(k_open + 1)).astype(bf16)
+        spread_x(2 * l + 1)
+        take_x(2 * l + 1)
+        weight(4, l)
+        for c in range(nd):
+            part = None
+            for p in range(ratio):
+                v = jnp.dot(
+                    x_recv[2 * l + 1, p, c * chunk:(c + 1) * chunk],
+                    v_exit[l, p * cols:(p + 1) * cols],
+                    preferred_element_type=f32,
+                )
+                part = v if part is None else part + v
+            row_send[k_open + 2, c] = part.astype(bf16)
+            send_row(k_open + 2, c)
+        residual = (residual.astype(f32) + row_sum(k_open + 2)).astype(bf16)
+    x_src[2 * layers] = residual
+    for c in range(nd):
+        send(
+            x_src.at[2 * layers], fin_recv.at[pl.ds(d * chunk, chunk)],
+            f_ss.at[c], f_rs.at[d], c, t, d == c,
+        )
+    for l in range(layers):
+        for s in range(nd):
+            arrive(nst_recv.at[s, l], n_rs.at[l, s])
+            for part in range(2):
+                out_state[l, part, :, s * own_ch:(s + 1) * own_ch] = nst_recv[s, l, part]
+    for s in range(nd):
+        arrive(fin_recv.at[pl.ds(s * chunk, chunk)], f_rs.at[s])
+    spread = jnp.dot(unpack_own[...], fin_recv[...], preferred_element_type=f32)
+    out_tok[...] = jnp.where(keep[...] > 0.5, spread, tok[...].astype(f32)).astype(bf16)
+    for far, is_self in pending:
+        if is_self is None:
+            far.wait_send()
+        else:
+            pl.when(jnp.logical_not(is_self))(far.wait_send)
+
+
+def fused_shards(
+    tokens, lengths, norm_gains, drive_proj, open_proj, glu_proj, merge_proj, exit_proj,
+    decay_rate, turn_rate, group_step_width, state_in, state_out, skip_gain, carried_state,
+):
+    f32, bf16 = jnp.float32, jnp.bfloat16
+    nd, nt = lax.axis_size("dp"), lax.axis_size("tp")
+    d, t = lax.axis_index("dp"), lax.axis_index("tp")
+    layers = norm_gains.shape[0]
+    own, steps, cols = tokens.shape
+    batch = own * nd
+    rows = 3 * batch
+    model = cols * nt
+    ratio = nt // nd
+    groups_own = decay_rate.shape[1]
+    few = groups_own // nd
+    entries = decay_rate.shape[2]
+    members = state_in.shape[-1]
+    width = few * members
+    own_ch = few * entries
+    chunk = rows // nd
+
+    everyone = lax.all_gather(lengths, "dp", axis=0, tiled=True)
+    starts = jnp.cumsum(everyone) - everyone
+    slot = jnp.arange(steps, dtype=jnp.int32)
+    where_tb = jnp.where(
+        slot[:, None] < everyone[None, :], starts[None, :] + slot[:, None], -1
+    ).reshape(steps * batch)
+    own_starts = lax.dynamic_slice_in_dim(starts, d * own, own, 0)
+    where_own = jnp.where(
+        slot[None, :] < lengths[:, None], own_starts[:, None] + slot[None, :], -1
+    ).reshape(own * steps)
+    index = jnp.arange(rows, dtype=jnp.int32)
+    unpack = (where_tb[:, None] == index[None, :]).astype(bf16)
+    pack = (index[:, None] == where_tb[None, :]).astype(bf16)
+    unpack_own = (where_own[:, None] == index[None, :]).astype(bf16)
+    pack_own = (index[:, None] == where_own[None, :]).astype(bf16)
+    keep = (where_own >= 0).astype(f32)[:, None]
+    gains = lax.dynamic_slice_in_dim(norm_gains, d * (model // nd), model // nd, 1).reshape(
+        layers, ratio, 1, cols
+    )
+
+    def mine(v, axis):
+        return lax.dynamic_slice_in_dim(v, d * few, few, axis)
+
+    real_eig = -mine(decay_rate, 1)
+    turn_now = mine(turn_rate, 1)
+    step_len = mine(group_step_width, 1)[..., None]
+    in_pair, out_pair = mine(state_in, 2), mine(state_out, 2)
+    skip_now = mine(skip_gain.reshape(layers, groups_own, members), 1).reshape(layers, 1, width)
+    magnitude = jnp.exp(step_len * real_eig)
+    decay_real = magnitude * jnp.cos(step_len * turn_now)
+    decay_imag = magnitude * jnp.sin(step_len * turn_now)
+    divisor = real_eig * real_eig + turn_now * turn_now
+    hold_real = ((decay_real - 1.0) * real_eig + decay_imag * turn_now) / divisor
+    hold_imag = (decay_imag * real_eig - (decay_real - 1.0) * turn_now) / divisor
+    inject_real = hold_real[..., None] * in_pair[:, 0] - hold_imag[..., None] * in_pair[:, 1]
+    inject_imag = hold_real[..., None] * in_pair[:, 1] + hold_imag[..., None] * in_pair[:, 0]
+    eye = jnp.eye(few, dtype=f32)
+    both = jnp.stack([inject_real, inject_imag], axis=1)
+    inject = (
+        jnp.transpose(both, (0, 2, 4, 1, 3))[:, :, :, :, None, :]
+        * eye[None, :, None, None, :, None]
+    ).reshape(layers, width, 2 * own_ch)
+    inject = jnp.pad(inject, ((0, 0), (0, width), (0, 0))).astype(bf16)
+    signed = jnp.stack([out_pair[:, 0], -out_pair[:, 1]], axis=1)
+    outmix = (
+        jnp.transpose(signed, (0, 1, 2, 4, 3))[:, :, :, :, None, :]
+        * eye[None, None, :, None, :, None]
+    ).reshape(layers, 2 * own_ch, width)
+    outmix = jnp.pad(outmix, ((0, 0), (0, 0), (0, width))).astype(bf16)
+    skip = jnp.pad(skip_now, ((0, 0), (0, 0), (0, width)))
+    decay = jnp.stack([decay_real, decay_imag], axis=1).reshape(layers, 2, 1, own_ch)
+
+    n_row = 1 + 3 * layers
+    half = rows // 2
+    vm = pltpu.VMEM
+    dma = pltpu.SemaphoreType.DMA
+    weights = (drive_proj, open_proj, glu_proj, merge_proj, exit_proj)
+    scratch = [vm(w.shape, bf16) for w in weights] + [
+        vm((n_row, nd, chunk, cols), bf16),
+        vm((n_row, nd, chunk, cols), bf16),
+        vm((layers, nd, rows, 2 * width), bf16),
+        vm((layers, nd, rows, 2 * width), bf16),
+        vm((layers, nd, half, 2 * width), bf16),
+        vm((layers, nd, half, 2 * width), bf16),
+        vm((2 * layers + 1, chunk, cols), bf16),
+        vm((2 * layers, ratio, rows, cols), bf16),
+        vm((2 * layers, half, 2 * width), bf16),
+        vm((2 * layers, nt, half, 2 * width), bf16),
+        vm((nd, layers, 2, own, own_ch), f32),
+        vm((layers, 2, batch, own_ch), f32),
+        vm((nd, layers, 2, own, own_ch), f32),
+        vm((rows, cols), bf16),
+        vm((rows, 128), f32),
+        vm((chunk, cols), f32),
+        vm((steps * batch, 2 * width), bf16),
+        dma((5, layers)),
+        dma((n_row, nd)), dma((n_row, nd)),
+        dma((layers, nd)), dma((layers, nd)),
+        dma((layers, nd)), dma((layers, nd)),
+        dma((2 * layers, nt)), dma((2 * layers, nt)),
+        dma((2 * layers, nt)), dma((2 * layers, nt)),
+        dma((nd,)), dma((nd,)),
+        dma((layers, nd)), dma((layers, nd)),
+        dma((nd,)), dma((nd,)),
+    ]
+    inside = pl.BlockSpec(memory_space=pltpu.VMEM)
+    outside = pl.BlockSpec(memory_space=pl.ANY)
+    out_rows, out_state = pl.pallas_call(
+        functools.partial(fused_kernel, (layers, nd, nt, rows, model)),
+        out_shape=(
+            jax.ShapeDtypeStruct((own * steps, cols), bf16),
+            jax.ShapeDtypeStruct(carried_state.shape, f32),
+        ),
+        in_specs=[inside] * 12 + [outside] * 5,
+        out_specs=(inside, inside),
+        scratch_shapes=scratch,
+        compiler_params=pltpu.CompilerParams(
+            collective_id=0, has_side_effects=True, vmem_limit_bytes=60 * 1024 * 1024
+        ),
+    )(
+        tokens.reshape(own * steps, cols), pack_own, unpack_own, keep, unpack, pack,
+        gains, decay, inject, outmix, skip, carried_state, *weights,
+    )
+    return out_rows.reshape(own, steps, cols), out_state
+
+
 def solution(mesh):
     in_specs = (
         P("dp", None, "tp"),
@@ -147,4 +543,12 @@
         P(None, None, "dp", "tp"),
     )
     out_specs = (P("dp", None, "tp"), P(None, None, "dp", "tp"))
-    return jax.shard_map(shards, mesh=mesh, in_specs=in_specs, out_specs=out_specs, check_vma=False)
+    ways, nd = mesh.shape["tp"], mesh.shape["dp"]
+
+    def run(*args):
+        groups = args[8].shape[1] // ways
+        whole_groups = groups % nd == 0 and ways % nd == 0
+        body = fused_shards if whole_groups else shards
+        return jax.shard_map(body, mesh=mesh, in_specs=in_specs, out_specs=out_specs, check_vma=False)(*args)
+
+    return run

time: 718 us -> 220 us (0.31)
  the two profiles are of different devices: /device:TPU:0 before, /device:TPU:23 now
where the time goes in v1:
time: 220 us; the launch traced here: 219 us
  Pallas kernels  192 us (87%)
  local copies, waits for them, and re-layouts  13 us (6%)
  other arithmetic  9.46 us (4%)
  blocking collectives  3.23 us (1%)
    pallas_call x1, Pallas kernels, fused_shards(): pl.pallas_call(functools.partial(fused_kernel, (layers, nd, nt, rows, mod...  192 us
    unnamed x7, local copies, waits for them, and re-layouts  5.67 us

profile of v1, /device:TPU:23, one launch (start us, length us, event | category | flops | bytes accessed | tf_op | source)
XLA Modules:
  0.0 219.3 jit_solution(6629424042468888214)
XLA Ops:
  0.7 1.2 dynamic-slice
  2.6 0.9 dynamic-update-slice
  3.4 3.2 %all-reduce.3 = s32[128]{0:T(128)S(1)} all-reduce(s32[128]{0:T(128)S(1)} %dynamic-update-slice), channel_id=1, replica_groups=mesh['tp'=8,'dp'=4] {'dp'}, use_global_device_ids=true, to_apply=%add.3 | all-reduce | flops 128 | bytes 1024
  6.6 0.7 constant_dynamic-slice_fusion.2
  7.5 0.6 reshape.249.gains
  8.1 0.8 add_divide_fusion
  9.0 0.7 subtract_divide_fusion
  9.9 0.6 pad_maximum_fusion.decay
  10.5 0.8 reshape.250
  11.3 0.6 pad.16.skip
  12.4 0.7 compare_convert_fusion
  13.1 0.7 add_select_fusion
  13.9 0.8 reshape.259.keep
  14.7 0.9 multiply_subtract_fusion
  15.7 0.9 constant_dynamic-slice_fusion
  16.7 0.8 fusion.3.unpack_own
  17.5 0.7 fusion.2.pack_own
  19.5 0.8 pad.15.outmix
  20.7 0.7 pad.14.inject
  21.4 1.1 fusion.1.pack
  22.5 1.1 fusion.unpack
  23.6 192.1 %shard_map.158 = (bf16[256,512]{1,0:T(8,128)(2,1)}, f32[2,2,32,1024]{3,2,1,0:T(8,128)}) custom-call(bf16[256,512]{1,0:T(8,128)(2,1)} %bitcast.15, bf16[384,256]{1,0:T(8,128)(2,1)} %fusion.2.pack_own, bf16[256,384]{1,0:T(8,128)(2,1)} %fusion.3.unpack_own, f32[256,1]{1,0:T(8,128)} %reshape.259.keep, bf16[1024,384]{1,0:T(8,128)(2,1)} %fusion.unpack, ...), custom_call_target="tpu_custom_call" | custom-call | tf_op jit(solution)/shard_map/pallas_call | solution.py:508
  215.8 1.7 copy.32
  217.4 1.9 copy.33
  (33 shorter events, 2.8 us)
Async XLA Ops:
  0.6 6.9 %copy-start = (f32[2,4096]{1,0:T(2,128)S(1)}, f32[2,4096]{1,0:T(2,128)}, u32[]{:S(2)}) copy-start(f32[2,4096]{1,0:T(2,128)} %param.17) | copy-start | bytes 98308

commit v2 on v1

--- a/solution.py
+++ b/solution.py
@@ -143,8 +143,9 @@
     w_sem, row_ss, row_rs, a_ss, a_rs, c_ss, c_rs, x_ss, x_rs, y_ss, y_rs,
     st_ss, st_rs, n_ss, n_rs, f_ss, f_rs,
 ):
-    layers, nd, nt, rows, model = dims
+    layers, nd, nt, all_rows, model, lots = dims
     ratio = nt // nd
+    rows = all_rows // lots
     chunk = rows // nd
     half = rows // 2
     f32, bf16 = jnp.float32, jnp.bfloat16
@@ -222,32 +223,59 @@
 
     def spread_x(k):
         slot = place * nd + d
-        for j in range(nt):
-            to = lax.rem(t + j, nt)
+        for j in range(nd):
+            to = lax.rem(home + j, nd) * ratio + place
             send(
                 x_src.at[k], x_recv.at[k, place, pl.ds(d * chunk, chunk)],
                 x_ss.at[k, j], x_rs.at[k, slot], home, to, (d == home) if j == 0 else None,
             )
 
+    def forward_x(k):
+        for s in range(nd):
+            piece = x_recv.at[k, place, pl.ds(s * chunk, chunk)]
+            arrive(piece, x_rs.at[k, place * nd + s])
+            for i in range(1, ratio):
+                to = home * ratio + lax.rem(place + i, ratio)
+                send(
+                    piece, piece, x_ss.at[k, nd + s * (ratio - 1) + i - 1],
+                    x_rs.at[k, place * nd + s], d, to, None,
+                )
+
     def take_x(k):
-        for p in range(ratio):
+        for i in range(1, ratio):
+            p = lax.rem(place + i, ratio)
             for s in range(nd):
                 arrive(x_recv.at[k, p, pl.ds(s * chunk, chunk)], x_rs.at[k, p * nd + s])
 
     def spread_y(k):
         slot = place * nd + d
-        for j in range(nt):
-            to = lax.rem(t + j, nt)
+        for j in range(nd):
+            to = lax.rem(home + j, nd) * ratio + place
             send(
                 y_src.at[k], y_recv.at[k, slot],
                 y_ss.at[k, j], y_rs.at[k, slot], home, to, (d == home) if j == 0 else None,
             )
 
+    def forward_y(k):
+        for s in range(nd):
+            slot = place * nd + s
+            piece = y_recv.at[k, slot]
+            arrive(piece, y_rs.at[k, slot])
+            for i in range(1, ratio):
+                to = home * ratio + lax.rem(place + i, ratio)
+                send(
+                    piece, piece, y_ss.at[k, nd + s * (ratio - 1) + i - 1],
+                    y_rs.at[k, slot], d, to, None,
+                )
+
     def take_y(k):
+        for i in range(1, ratio):
+            p = lax.rem(place + i, ratio)
+            for s in range(nd):
+                arrive(y_recv.at[k, p * nd + s], y_rs.at[k, p * nd + s])
         parts = []
         for p in range(ratio):
             for s in range(nd):
-                arrive(y_recv.at[k, p * nd + s], y_rs.at[k, p * nd + s])
                 v = y_recv[k, p * nd + s]
                 parts.append(jnp.concatenate([v[:, :width], v[:, width:]], axis=0))
         return jnp.concatenate(parts, axis=1)
@@ -255,63 +283,79 @@
     def fold(v):
         return jnp.concatenate([v[:half], v[half:]], axis=1)
 
-    for c in range(nd):
-        part = jnp.dot(pack_own[c * chunk:(c + 1) * chunk, :], tok[...], preferred_element_type=f32)
-        row_send[0, c] = part.astype(bf16)
-        send_row(0, c)
+    every = range(lots)
+    for h in every:
+        for c in range(nd):
+            top = h * rows + c * chunk
+            part = jnp.dot(pack_own[top:top + chunk, :], tok[...], preferred_element_type=f32)
+            row_send[h, c] = part.astype(bf16)
+            send_row(h, c)
     for c in range(nd):
         send(
             carried.at[:, :, :, pl.ds(c * own_ch, own_ch)], st_recv.at[d],
             st_ss.at[c], st_rs.at[d], c, t, d == c,
         )
-    residual = row_sum(0).astype(bf16)
     cols = tok.shape[1]
+    residual = []
+    for h in every:
+        residual.append(row_sum(h).astype(bf16))
+        x_src[h] = residual[h]
+        spread_x(h)
+    for s in range(nd):
+        arrive(st_recv.at[s], st_rs.at[s])
     for l in range(layers):
-        x_src[2 * l] = residual
-        spread_x(2 * l)
-        if l == 0:
+        first, second = 2 * l * lots, (2 * l + 1) * lots
+        k_open = (1 + 3 * l) * lots
+        k_merge, k_exit = k_open + lots, k_open + 2 * lots
+        for h in every:
+            forward_x(first + h)
+        weight(0, l)
+        normed = []
+        for h in every:
+            take_x(first + h)
+            scaled, squares = [], None
+            for p in range(ratio):
+                raw = x_recv[first + h, p].astype(f32)
+                sq = jnp.sum(raw * raw, axis=1, keepdims=True)
+                squares = sq if squares is None else squares + sq
+                scaled.append((raw * gains[l, p]).astype(bf16))
+            normed.append(jnp.concatenate(scaled, axis=1))
+            drive = jnp.dot(normed[h], v_drive[l], preferred_element_type=f32)
+            high = squares.astype(bf16)
+            low = (squares - high.astype(f32)).astype(bf16)
+            lane = lax.broadcasted_iota(jnp.int32, (rows, width), 1)
+            tail = jnp.where(
+                lane == 0, high.astype(f32), jnp.where(lane == 1, low.astype(f32), 0.0)
+            ).astype(bf16)
+            k = l * lots + h
+            for c in range(nd):
+                a_send[k, c] = jnp.concatenate(
+                    [drive[:, c * width:(c + 1) * width].astype(bf16), tail], axis=1
+                )
+                send(a_send.at[k, c], a_recv.at[k, d], a_ss.at[k, c], a_rs.at[k, d], c, t, d == c)
+        weight(1, l)
+        for h in every:
+            for c in range(nd):
+                part = jnp.dot(
+                    normed[h][c * chunk:(c + 1) * chunk], v_open[l], preferred_element_type=f32
+                )
+                row_send[k_open + h, c] = part.astype(bf16)
+                send_row(k_open + h, c)
+        feeds = []
+        for h in every:
+            k = l * lots + h
+            summed = None
             for s in range(nd):
-                arrive(st_recv.at[s], st_rs.at[s])
-        take_x(2 * l)
-        scaled, squares = [], None
-        for p in range(ratio):
-            raw = x_recv[2 * l, p].astype(f32)
-            sq = jnp.sum(raw * raw, axis=1, keepdims=True)
-            squares = sq if squares is None else squares + sq
-            scaled.append((raw * gains[l, p]).astype(bf16))
-        normed = jnp.concatenate(scaled, axis=1)
-        weight(0, l)
-        drive = jnp.dot(normed, v_drive[l], preferred_element_type=f32)
-        high = squares.astype(bf16)
-        low = (squares - high.astype(f32)).astype(bf16)
-        lane = lax.broadcasted_iota(jnp.int32, (rows, width), 1)
-        tail = jnp.where(
-            lane == 0, high.astype(f32), jnp.where(lane == 1, low.astype(f32), 0.0)
-        ).astype(bf16)
-        for c in range(nd):
-            a_send[l, c] = jnp.concatenate(
-                [drive[:, c * width:(c + 1) * width].astype(bf16), tail], axis=1
-            )
-            send(a_send.at[l, c], a_recv.at[l, d], a_ss.at[l, c], a_rs.at[l, d], c, t, d == c)
-        weight(1, l)
-        k_open = 1 + 3 * l
-        for c in range(nd):
-            part = jnp.dot(
-                normed[c * chunk:(c + 1) * chunk], v_open[l], preferred_element_type=f32
-            )
-            row_send[k_open, c] = part.astype(bf16)
-            send_row(k_open, c)
-        summed = None
-        for s in range(nd):
-            arrive(a_recv.at[l, s], a_rs.at[l, s])
-            v = a_recv[l, s].astype(f32)
-            summed = v if summed is None else summed + v
-        full_sq = summed[:, width:width + 1] + summed[:, width + 1:width + 2]
-        inverse = lax.rsqrt(full_sq / model + EPS)
-        inv_buf[...] = jnp.broadcast_to(inverse, inv_buf.shape)
-        lane2 = lax.broadcasted_iota(jnp.int32, summed.shape, 1)
-        feed = jnp.where(lane2 < width, summed * inverse, jnp.where(lane2 == width, 1.0, 0.0))
-        feed = feed.astype(bf16)
+                arrive(a_recv.at[k, s], a_rs.at[k, s])
+                v = a_recv[k, s].astype(f32)
+                summed = v if summed is None else summed + v
+            full_sq = summed[:, width:width + 1] + summed[:, width + 1:width + 2]
+            inverse = lax.rsqrt(full_sq / model + EPS)
+            inv_buf[h * rows:(h + 1) * rows, :] = jnp.broadcast_to(inverse, (rows, 128))
+            lane2 = lax.broadcasted_iota(jnp.int32, summed.shape, 1)
+            feed = jnp.where(lane2 < width, summed * inverse, jnp.where(lane2 == width, 1.0, 0.0))
+            feeds.append(feed.astype(bf16))
+        feed = jnp.concatenate(feeds, axis=0)
         real = jnp.concatenate([st_recv[s, l, 0] for s in range(nd)], axis=0)
         imag = jnp.concatenate([st_recv[s, l, 1] for s in range(nd)], axis=0)
         dr, di = decay[l, 0], decay[l, 1]
@@ -329,65 +373,92 @@
             act_buf[span, :] = jax.nn.gelu(read).astype(bf16)
         st_new[l, 0] = real
         st_new[l, 1] = imag
-        packed = jnp.dot(pack[...], act_buf[...], preferred_element_type=f32).astype(bf16)
-        activated = fold(packed[:, :width])
-        y_src[2 * l] = activated
-        spread_y(2 * l)
+        activated = []
+        for h in every:
+            packed = jnp.dot(
+                pack[h * rows:(h + 1) * rows, :], act_buf[...], preferred_element_type=f32
+            ).astype(bf16)
+            activated.append(fold(packed[:, :width]))
+            y_src[first + h] = activated[h]
+            spread_y(first + h)
+        for h in every:
+            mine = pl.ds(pl.multiple_of(h * rows + d * chunk, chunk), chunk)
+            gate_buf[h] = jax.nn.sigmoid(row_sum(k_open + h) * inv_buf[mine, 0:1])
+        weight(2, l)
+        for h in every:
+            forward_y(first + h)
+        for h in every:
+            wide = take_y(first + h)
+            gating = jnp.dot(wide, v_glu[l], preferred_element_type=f32).astype(bf16)
+            k = l * lots + h
+            for c in range(nd):
+                c_send[k, c] = fold(gating[:, c * width:(c + 1) * width])
+                send(c_send.at[k, c], c_recv.at[k, d], c_ss.at[k, c], c_rs.at[k, d], c, t, d == c)
+        for h in every:
+            k = l * lots + h
+            summed = None
+            for s in range(nd):
+                arrive(c_recv.at[k, s], c_rs.at[k, s])
+                v = c_recv[k, s].astype(f32)
+                summed = v if summed is None else summed + v
+            gated = activated[h].astype(f32) * jax.nn.sigmoid(summed)
+            y_src[second + h] = gated.astype(bf16)
+            spread_y(second + h)
+        weight(3, l)
+        for h in every:
+            forward_y(second + h)
+        for h in every:
+            wide = take_y(second + h)
+            for c in range(nd):
+                part = jnp.dot(
+                    wide[c * chunk:(c + 1) * chunk], v_merge[l], preferred_element_type=f32
+                )
+                row_send[k_merge + h, c] = part.astype(bf16)
+                send_row(k_merge + h, c)
+        for h in every:
+            x_src[second + h] = (gate_buf[h] * row_sum(k_merge + h)).astype(bf16)
+            spread_x(second + h)
         for c in range(nd):
             send(
                 st_new.at[l, :, pl.ds(c * batch_own, batch_own)], nst_recv.at[d, l],
                 n_ss.at[l, c], n_rs.at[l, d], c, t, d == c,
             )
-        mine = pl.ds(pl.multiple_of(d * chunk, chunk), chunk)
-        gate_buf[...] = jax.nn.sigmoid(row_sum(k_open) * inv_buf[mine, 0:1])
-        wide = take_y(2 * l)
-        weight(2, l)
-        gating = jnp.dot(wide, v_glu[l], preferred_element_type=f32).astype(bf16)
-        for c in range(nd):
-            c_send[l, c] = fold(gating[:, c * width:(c + 1) * width])
-            send(c_send.at[l, c], c_recv.at[l, d], c_ss.at[l, c], c_rs.at[l, d], c, t, d == c)
-        summed = None
-        for s in range(nd):
-            arrive(c_recv.at[l, s], c_rs.at[l, s])
-            v = c_recv[l, s].astype(f32)
-            summed = v if summed is None else summed + v
-        y_src[2 * l + 1] = (activated.astype(f32) * jax.nn.sigmoid(summed)).astype(bf16)
-        spread_y(2 * l + 1)
-        wide = take_y(2 * l + 1)
-        weight(3, l)
-        for c in range(nd):
-            part = jnp.dot(wide[c * chunk:(c + 1) * chunk], v_merge[l], preferred_element_type=f32)
-            row_send[k_open + 1, c] = part.astype(bf16)
-            send_row(k_open + 1, c)
-        x_src[2 * l + 1] = (gate_buf[...] * row_sum(k_open + 1)).astype(bf16)
-        spread_x(2 * l + 1)
-        take_x(2 * l + 1)
         weight(4, l)
-        for c in range(nd):
-            part = None
-            for p in range(ratio):
-                v = jnp.dot(
-                    x_recv[2 * l + 1, p, c * chunk:(c + 1) * chunk],
-                    v_exit[l, p * cols:(p + 1) * cols],
-                    preferred_element_type=f32,
-                )
-                part = v if part is None else part + v
-            row_send[k_open + 2, c] = part.astype(bf16)
-            send_row(k_open + 2, c)
-        residual = (residual.astype(f32) + row_sum(k_open + 2)).astype(bf16)
-    x_src[2 * layers] = residual
-    for c in range(nd):
-        send(
-            x_src.at[2 * layers], fin_recv.at[pl.ds(d * chunk, chunk)],
-            f_ss.at[c], f_rs.at[d], c, t, d == c,
-        )
+        for h in every:
+            forward_x(second + h)
+        for h in every:
+            take_x(second + h)
+            for c in range(nd):
+                part = None
+                for p in range(ratio):
+                    v = jnp.dot(
+                        x_recv[second + h, p, c * chunk:(c + 1) * chunk],
+                        v_exit[l, p * cols:(p + 1) * cols],
+                        preferred_element_type=f32,
+                    )
+                    part = v if part is None else part + v
+                row_send[k_exit + h, c] = part.astype(bf16)
+                send_row(k_exit + h, c)
+        for h in every:
+            residual[h] = (residual[h].astype(f32) + row_sum(k_exit + h)).astype(bf16)
+            k = (2 * l + 2) * lots + h
+            x_src[k] = residual[h]
+            if l + 1 < layers:
+                spread_x(k)
+            else:
+                for c in range(nd):
+                    send(
+                        x_src.at[k], fin_recv.at[pl.ds(h * rows + d * chunk, chunk)],
+                        f_ss.at[h, c], f_rs.at[h, d], c, t, d == c,
+                    )
     for l in range(layers):
         for s in range(nd):
             arrive(nst_recv.at[s, l], n_rs.at[l, s])
             for part in range(2):
                 out_state[l, part, :, s * own_ch:(s + 1) * own_ch] = nst_recv[s, l, part]
-    for s in range(nd):
-        arrive(fin_recv.at[pl.ds(s * chunk, chunk)], f_rs.at[s])
+    for h in every:
+        for s in range(nd):
+            arrive(fin_recv.at[pl.ds(h * rows + s * chunk, chunk)], f_rs.at[h, s])
     spread = jnp.dot(unpack_own[...], fin_recv[...], preferred_element_type=f32)
     out_tok[...] = jnp.where(keep[...] > 0.5, spread, tok[...].astype(f32)).astype(bf16)
     for far, is_self in pending:
@@ -470,43 +541,48 @@
     skip = jnp.pad(skip_now, ((0, 0), (0, 0), (0, width)))
     decay = jnp.stack([decay_real, decay_imag], axis=1).reshape(layers, 2, 1, own_ch)
 
-    n_row = 1 + 3 * layers
-    half = rows // 2
+    lots = 2
+    n_row = (1 + 3 * layers) * lots
+    n_col = layers * lots
+    n_all = 2 * layers * lots
+    lot = rows // lots
+    piece = chunk // lots
+    half = lot // 2
     vm = pltpu.VMEM
     dma = pltpu.SemaphoreType.DMA
     weights = (drive_proj, open_proj, glu_proj, merge_proj, exit_proj)
     scratch = [vm(w.shape, bf16) for w in weights] + [
-        vm((n_row, nd, chunk, cols), bf16),
-        vm((n_row, nd, chunk, cols), bf16),
-        vm((layers, nd, rows, 2 * width), bf16),
-        vm((layers, nd, rows, 2 * width), bf16),
-        vm((layers, nd, half, 2 * width), bf16),
-        vm((layers, nd, half, 2 * width), bf16),
-        vm((2 * layers + 1, chunk, cols), bf16),
-        vm((2 * layers, ratio, rows, cols), bf16),
-        vm((2 * layers, half, 2 * width), bf16),
-        vm((2 * layers, nt, half, 2 * width), bf16),
+        vm((n_row, nd, piece, cols), bf16),
+        vm((n_row, nd, piece, cols), bf16),
+        vm((n_col, nd, lot, 2 * width), bf16),
+        vm((n_col, nd, lot, 2 * width), bf16),
+        vm((n_col, nd, half, 2 * width), bf16),
+        vm((n_col, nd, half, 2 * width), bf16),
+        vm((n_all + lots, piece, cols), bf16),
+        vm((n_all, ratio, lot, cols), bf16),
+        vm((n_all, half, 2 * width), bf16),
+        vm((n_all, nt, half, 2 * width), bf16),
         vm((nd, layers, 2, own, own_ch), f32),
         vm((layers, 2, batch, own_ch), f32),
         vm((nd, layers, 2, own, own_ch), f32),
         vm((rows, cols), bf16),
         vm((rows, 128), f32),
-        vm((chunk, cols), f32),
+        vm((lots, piece, cols), f32),
         vm((steps * batch, 2 * width), bf16),
         dma((5, layers)),
         dma((n_row, nd)), dma((n_row, nd)),
-        dma((layers, nd)), dma((layers, nd)),
-        dma((layers, nd)), dma((layers, nd)),
-        dma((2 * layers, nt)), dma((2 * layers, nt)),
-        dma((2 * layers, nt)), dma((2 * layers, nt)),
+        dma((n_col, nd)), dma((n_col, nd)),
+        dma((n_col, nd)), dma((n_col, nd)),
+        dma((n_all, nd * ratio)), dma((n_all, nt)),
+        dma((n_all, nd * ratio)), dma((n_all, nt)),
         dma((nd,)), dma((nd,)),
         dma((layers, nd)), dma((layers, nd)),
-        dma((nd,)), dma((nd,)),
+        dma((lots, nd)), dma((lots, nd)),
     ]
     inside = pl.BlockSpec(memory_space=pltpu.VMEM)
     outside = pl.BlockSpec(memory_space=pl.ANY)
     out_rows, out_state = pl.pallas_call(
-        functools.partial(fused_kernel, (layers, nd, nt, rows, model)),
+        functools.partial(fused_kernel, (layers, nd, nt, rows, model, lots)),
         out_shape=(
             jax.ShapeDtypeStruct((own * steps, cols), bf16),
             jax.ShapeDtypeStruct(carried_state.shape, f32),

time: 220 us -> 183 us (0.83)
  the two profiles are of different devices: /device:TPU:23 before, /device:TPU:0 now
where the time goes in v2:
time: 183 us; the launch traced here: 181 us
  Pallas kernels  151 us (83%)
  local copies, waits for them, and re-layouts  13 us (7%)
  other arithmetic  9.46 us (5%)
  blocking collectives  6.41 us (4%)
    pallas_call x1, Pallas kernels, fused_shards(): pl.pallas_call(functools.partial(fused_kernel, (layers, nd, nt, rows, mod...  151 us
    unnamed x1, blocking collectives  6.41 us
    unnamed x7, local copies, waits for them, and re-layouts  5.67 us

profile of v2, /device:TPU:0, one launch (start us, length us, event | category | flops | bytes accessed | tf_op | source)
XLA Modules:
  0.0 181.1 jit_solution(11426074076160572142)
XLA Ops:
  0.7 1.2 dynamic-slice
  2.6 0.9 dynamic-update-slice
  3.4 6.4 %all-reduce.3 = s32[128]{0:T(128)S(1)} all-reduce(s32[128]{0:T(128)S(1)} %dynamic-update-slice), channel_id=1, replica_groups=mesh['tp'=8,'dp'=4] {'dp'}, use_global_device_ids=true, to_apply=%add.3 | all-reduce | flops 128 | bytes 1024
  9.8 0.7 constant_dynamic-slice_fusion.2
  10.7 0.6 reshape.249.gains
  11.3 0.8 add_divide_fusion
  12.2 0.7 subtract_divide_fusion
  13.0 0.6 pad_maximum_fusion.decay
  13.6 0.8 reshape.250
  14.5 0.6 pad.16.skip
  15.5 0.7 compare_convert_fusion
  16.3 0.7 add_select_fusion
  17.1 0.8 reshape.259.keep
  17.9 0.9 multiply_subtract_fusion
  18.9 0.9 constant_dynamic-slice_fusion
  19.9 0.8 fusion.3.unpack_own
  20.6 0.7 fusion.2.pack_own
  22.7 0.8 pad.15.outmix
  23.9 0.7 pad.14.inject
  24.6 1.1 fusion.1.pack
  25.7 1.1 fusion.unpack
  26.8 150.8 %shard_map.158 = (bf16[256,512]{1,0:T(8,128)(2,1)}, f32[2,2,32,1024]{3,2,1,0:T(8,128)}) custom-call(bf16[256,512]{1,0:T(8,128)(2,1)} %bitcast.15, bf16[384,256]{1,0:T(8,128)(2,1)} %fusion.2.pack_own, bf16[256,384]{1,0:T(8,128)(2,1)} %fusion.3.unpack_own, f32[256,1]{1,0:T(8,128)} %reshape.259.keep, bf16[1024,384]{1,0:T(8,128)(2,1)} %fusion.unpack, ...), custom_call_target="tpu_custom_call" | custom-call | tf_op jit(solution)/shard_map/pallas_call | solution.py:584
  177.6 1.7 copy.32
  179.3 1.9 %copy.33 = f32[2,2,32,1024]{3,2,1,0:T(8,128)} copy(f32[2,2,32,1024]{3,2,1,0:T(8,128)} %get-tuple-element.16) | data formatting | bytes 1048576
  (33 shorter events, 2.8 us)
Async XLA Ops:
  0.6 10.0 %copy-start = (f32[2,4096]{1,0:T(2,128)S(1)}, f32[2,4096]{1,0:T(2,128)}, u32[]{:S(2)}) copy-start(f32[2,4096]{1,0:T(2,128)} %param.17) | copy-start | bytes 98308

commit v3 on v2

--- a/solution.py
+++ b/solution.py
@@ -133,15 +133,15 @@
 
 def fused_kernel(
     dims,
-    tok, pack_own, unpack_own, keep, unpack, pack, gains, decay, inject, outmix, skip, carried,
+    tok, lens, gains, decay, inject, outmix, skip, carried,
     w_drive, w_open, w_glu, w_merge, w_exit,
     out_tok, out_state,
     v_drive, v_open, v_glu, v_merge, v_exit,
     row_send, row_recv, a_send, a_recv, c_send, c_recv,
     x_src, x_recv, y_src, y_recv, st_recv, st_new, nst_recv, fin_recv,
-    inv_buf, gate_buf, act_buf,
+    inv_buf, gate_buf, act_buf, len_recv, pack_own, unpack,
     w_sem, row_ss, row_rs, a_ss, a_rs, c_ss, c_rs, x_ss, x_rs, y_ss, y_rs,
-    st_ss, st_rs, n_ss, n_rs, f_ss, f_rs,
+    st_ss, st_rs, n_ss, n_rs, f_ss, f_rs, l_ss, l_rs,
 ):
     layers, nd, nt, all_rows, model, lots = dims
     ratio = nt // nd
@@ -155,9 +155,9 @@
     place = lax.rem(t, ratio)
     batch_own = carried.shape[2]
     batch = batch_own * nd
-    own_ch = inject.shape[2] // 2
+    own_ch = inject.shape[3] // 2
     width = c_send.shape[-1] // 2
-    steps = unpack.shape[0] // batch
+    steps = tok.shape[0] // batch_own
 
     loads = []
     for i, (src, dst) in enumerate(
@@ -282,6 +282,45 @@
 
     def fold(v):
         return jnp.concatenate([v[:half], v[half:]], axis=1)
+
+    for c in range(nd):
+        send(lens, len_recv.at[d], l_ss.at[c], l_rs.at[d], c, t, d == c)
+    len_row = None
+    for s in range(nd):
+        arrive(len_recv.at[s], l_rs.at[s])
+        len_row = len_recv[s] if len_row is None else len_row + len_recv[s]
+    down = lax.broadcasted_iota(jnp.int32, (batch, batch), 0)
+    along = lax.broadcasted_iota(jnp.int32, (batch, batch), 1)
+    before = jnp.where(down < along, 1.0, 0.0).astype(bf16)
+    start_row = jnp.dot(len_row.astype(bf16), before, preferred_element_type=f32)
+
+    def upright(v):
+        wide = jnp.broadcast_to(v[0:1], (batch, batch))
+        return jnp.sum(jnp.where(down == along, wide, 0.0), axis=1, keepdims=True)
+
+    len_col, start_col = upright(len_row), upright(start_row)
+    count = lax.broadcasted_iota(jnp.int32, (batch, all_rows), 1).astype(f32)
+    for step in range(steps):
+        hit = jnp.logical_and(count == start_col + step, len_col > step)
+        unpack[step * batch:(step + 1) * batch, :] = jnp.where(hit, 1.0, 0.0).astype(bf16)
+    own_rows = tok.shape[0]
+    local = lax.broadcasted_iota(jnp.int32, (batch, own_rows), 0) - d * batch_own
+    item = lax.broadcasted_iota(jnp.int32, (batch, own_rows), 1)
+    inside = jnp.logical_and(item >= local * steps, item < (local + 1) * steps)
+    expand = jnp.where(inside, 1.0, 0.0)
+    order = (lax.broadcasted_iota(jnp.int32, len_row.shape, 1) - d * batch_own).astype(f32)
+    exact = functools.partial(
+        jnp.dot, preferred_element_type=f32, precision=lax.Precision.HIGHEST
+    )
+    spot = exact(start_row - steps * order, expand)[0:1]
+    spot = spot + lax.broadcasted_iota(jnp.int32, (1, own_rows), 1).astype(f32)
+    end = exact(start_row + len_row, expand)[0:1]
+    spot = jnp.where(spot < end, spot, -1.0)
+    tall = lax.broadcasted_iota(jnp.int32, (all_rows, own_rows), 0).astype(f32)
+    pack_own[...] = jnp.where(tall == spot, 1.0, 0.0).astype(bf16)
+
+    def turned(a, b):
+        return lax.dot_general(a, b, (((0,), (0,)), ((), ())), preferred_element_type=f32)
 
     every = range(lots)
     for h in every:
@@ -318,7 +357,7 @@
                 raw = x_recv[first + h, p].astype(f32)
                 sq = jnp.sum(raw * raw, axis=1, keepdims=True)
                 squares = sq if squares is None else squares + sq
-                scaled.append((raw * gains[l, p]).astype(bf16))
+                scaled.append((raw * gains[l, d, p]).astype(bf16))
             normed.append(jnp.concatenate(scaled, axis=1))
             drive = jnp.dot(normed[h], v_drive[l], preferred_element_type=f32)
             high = squares.astype(bf16)
@@ -358,26 +397,25 @@
         feed = jnp.concatenate(feeds, axis=0)
         real = jnp.concatenate([st_recv[s, l, 0] for s in range(nd)], axis=0)
         imag = jnp.concatenate([st_recv[s, l, 1] for s in range(nd)], axis=0)
-        dr, di = decay[l, 0], decay[l, 1]
+        dr, di = decay[l, 0, d], decay[l, 1, d]
         for step in range(steps):
             span = slice(step * batch, (step + 1) * batch)
             u = jnp.dot(unpack[span, :], feed, preferred_element_type=f32)
             live = u[:, width:width + 1] > 0.5
-            push = jnp.dot(u.astype(bf16), inject[l], preferred_element_type=f32)
+            push = jnp.dot(u.astype(bf16), inject[l, d], preferred_element_type=f32)
             moved_real = dr * real - di * imag + push[:, :own_ch]
             moved_imag = dr * imag + di * real + push[:, own_ch:]
             real = jnp.where(live, moved_real, real)
             imag = jnp.where(live, moved_imag, imag)
             both = jnp.concatenate([real, imag], axis=1).astype(bf16)
-            read = jnp.dot(both, outmix[l], preferred_element_type=f32) + skip[l] * u
+            read = jnp.dot(both, outmix[l, d], preferred_element_type=f32) + skip[l, d] * u
             act_buf[span, :] = jax.nn.gelu(read).astype(bf16)
         st_new[l, 0] = real
         st_new[l, 1] = imag
+        packed_all = turned(unpack[...], act_buf[...]).astype(bf16)
         activated = []
         for h in every:
-            packed = jnp.dot(
-                pack[h * rows:(h + 1) * rows, :], act_buf[...], preferred_element_type=f32
-            ).astype(bf16)
+            packed = packed_all[h * rows:(h + 1) * rows]
             activated.append(fold(packed[:, :width]))
             y_src[first + h] = activated[h]
             spread_y(first + h)
@@ -459,8 +497,9 @@
     for h in every:
         for s in range(nd):
             arrive(fin_recv.at[pl.ds(h * rows + s * chunk, chunk)], f_rs.at[h, s])
-    spread = jnp.dot(unpack_own[...], fin_recv[...], preferred_element_type=f32)
-    out_tok[...] = jnp.where(keep[...] > 0.5, spread, tok[...].astype(f32)).astype(bf16)
+    spread = turned(pack_own[...], fin_recv[...])
+    keep = turned(pack_own[...], jnp.ones((all_rows, 128), bf16))[:, 0:1]
+    out_tok[...] = jnp.where(keep > 0.5, spread, tok[...].astype(f32)).astype(bf16)
     for far, is_self in pending:
         if is_self is None:
             far.wait_send()
@@ -489,34 +528,16 @@
     own_ch = few * entries
     chunk = rows // nd
 
-    everyone = lax.all_gather(lengths, "dp", axis=0, tiled=True)
-    starts = jnp.cumsum(everyone) - everyone
-    slot = jnp.arange(steps, dtype=jnp.int32)
-    where_tb = jnp.where(
-        slot[:, None] < everyone[None, :], starts[None, :] + slot[:, None], -1
-    ).reshape(steps * batch)
-    own_starts = lax.dynamic_slice_in_dim(starts, d * own, own, 0)
-    where_own = jnp.where(
-        slot[None, :] < lengths[:, None], own_starts[:, None] + slot[None, :], -1
-    ).reshape(own * steps)
-    index = jnp.arange(rows, dtype=jnp.int32)
-    unpack = (where_tb[:, None] == index[None, :]).astype(bf16)
-    pack = (index[:, None] == where_tb[None, :]).astype(bf16)
-    unpack_own = (where_own[:, None] == index[None, :]).astype(bf16)
-    pack_own = (index[:, None] == where_own[None, :]).astype(bf16)
-    keep = (where_own >= 0).astype(f32)[:, None]
-    gains = lax.dynamic_slice_in_dim(norm_gains, d * (model // nd), model // nd, 1).reshape(
-        layers, ratio, 1, cols
-    )
-
-    def mine(v, axis):
-        return lax.dynamic_slice_in_dim(v, d * few, few, axis)
-
-    real_eig = -mine(decay_rate, 1)
-    turn_now = mine(turn_rate, 1)
-    step_len = mine(group_step_width, 1)[..., None]
-    in_pair, out_pair = mine(state_in, 2), mine(state_out, 2)
-    skip_now = mine(skip_gain.reshape(layers, groups_own, members), 1).reshape(layers, 1, width)
+    place = jnp.arange(batch, dtype=jnp.int32) // own
+    lens = jnp.where(place == d, jnp.tile(lengths, nd), 0).astype(f32)
+    lens = jnp.broadcast_to(lens[None, :], (8, batch))
+    gains = norm_gains.reshape(layers, nd, ratio, 1, cols)
+
+    real_eig = -decay_rate
+    turn_now = turn_rate
+    step_len = group_step_width[..., None]
+    in_pair, out_pair = state_in, state_out
+    skip_now = skip_gain.reshape(layers, nd, 1, width)
     magnitude = jnp.exp(step_len * real_eig)
     decay_real = magnitude * jnp.cos(step_len * turn_now)
     decay_imag = magnitude * jnp.sin(step_len * turn_now)
@@ -526,22 +547,26 @@
     inject_real = hold_real[..., None] * in_pair[:, 0] - hold_imag[..., None] * in_pair[:, 1]
     inject_imag = hold_real[..., None] * in_pair[:, 1] + hold_imag[..., None] * in_pair[:, 0]
     eye = jnp.eye(few, dtype=f32)
-    both = jnp.stack([inject_real, inject_imag], axis=1)
+    both = jnp.stack([inject_real, inject_imag], axis=1).reshape(
+        layers, 2, nd, few, entries, members
+    )
     inject = (
-        jnp.transpose(both, (0, 2, 4, 1, 3))[:, :, :, :, None, :]
-        * eye[None, :, None, None, :, None]
-    ).reshape(layers, width, 2 * own_ch)
-    inject = jnp.pad(inject, ((0, 0), (0, width), (0, 0))).astype(bf16)
-    signed = jnp.stack([out_pair[:, 0], -out_pair[:, 1]], axis=1)
+        jnp.transpose(both, (0, 2, 3, 5, 1, 4))[:, :, :, :, :, None, :]
+        * eye[None, None, :, None, None, :, None]
+    ).reshape(layers, nd, width, 2 * own_ch)
+    inject = jnp.pad(inject, ((0, 0), (0, 0), (0, width), (0, 0))).astype(bf16)
+    signed = jnp.stack([out_pair[:, 0], -out_pair[:, 1]], axis=1).reshape(
+        layers, 2, nd, few, members, entries
+    )
     outmix = (
-        jnp.transpose(signed, (0, 1, 2, 4, 3))[:, :, :, :, None, :]
-        * eye[None, None, :, None, :, None]
-    ).reshape(layers, 2 * own_ch, width)
-    outmix = jnp.pad(outmix, ((0, 0), (0, 0), (0, width))).astype(bf16)
-    skip = jnp.pad(skip_now, ((0, 0), (0, 0), (0, width)))
-    decay = jnp.stack([decay_real, decay_imag], axis=1).reshape(layers, 2, 1, own_ch)
-
-    lots = 2
+        jnp.transpose(signed, (0, 2, 1, 3, 5, 4))[:, :, :, :, :, None, :]
+        * eye[None, None, None, :, None, :, None]
+    ).reshape(layers, nd, 2 * own_ch, width)
+    outmix = jnp.pad(outmix, ((0, 0), (0, 0), (0, 0), (0, width))).astype(bf16)
+    skip = jnp.pad(skip_now, ((0, 0), (0, 0), (0, 0), (0, width)))
+    decay = jnp.stack([decay_real, decay_imag], axis=1).reshape(layers, 2, nd, 1, own_ch)
+
+    lots = 3
     n_row = (1 + 3 * layers) * lots
     n_col = layers * lots
     n_all = 2 * layers * lots
@@ -569,6 +594,9 @@
         vm((rows, 128), f32),
         vm((lots, piece, cols), f32),
         vm((steps * batch, 2 * width), bf16),
+        vm((nd, 8, batch), f32),
+        vm((rows, own * steps), bf16),
+        vm((steps * batch, rows), bf16),
         dma((5, layers)),
         dma((n_row, nd)), dma((n_row, nd)),
         dma((n_col, nd)), dma((n_col, nd)),
@@ -578,6 +606,7 @@
         dma((nd,)), dma((nd,)),
         dma((layers, nd)), dma((layers, nd)),
         dma((lots, nd)), dma((lots, nd)),
+        dma((nd,)), dma((nd,)),
     ]
     inside = pl.BlockSpec(memory_space=pltpu.VMEM)
     outside = pl.BlockSpec(memory_space=pl.ANY)
@@ -587,14 +616,14 @@
             jax.ShapeDtypeStruct((own * steps, cols), bf16),
             jax.ShapeDtypeStruct(carried_state.shape, f32),
         ),
-        in_specs=[inside] * 12 + [outside] * 5,
+        in_specs=[inside] * 8 + [outside] * 5,
         out_specs=(inside, inside),
         scratch_shapes=scratch,
         compiler_params=pltpu.CompilerParams(
             collective_id=0, has_side_effects=True, vmem_limit_bytes=60 * 1024 * 1024
         ),
     )(
-        tokens.reshape(own * steps, cols), pack_own, unpack_own, keep, unpack, pack,
+        tokens.reshape(own * steps, cols), lens,
         gains, decay, inject, outmix, skip, carried_state, *weights,
     )
     return out_rows.reshape(own, steps, cols), out_state

time: 183 us -> 174 us (0.951)
  other arithmetic: 9.46 us -> 2.02 us
  blocking collectives: 6.41 us -> 0 us
  Pallas kernels: 151 us -> 155 us
  local copies, waits for them, and re-layouts: 13 us -> 16.5 us
    unnamed x1 -> x0, blocking collectives: 6.41 us -> none
    convert_element_type x5 -> x1, other arithmetic: 4.39 us -> 0.01 us  [fused_shards(): lens = jnp.where(place == d, jnp.tile(lengths, nd), 0).astype(f32)]
    pallas_call x1, Pallas kernels: 151 us -> 155 us  [fused_shards(): pl.pallas_call(functools.partial(fused_kernel, (layers, nd, nt, rows, mod...]
    mul x10, local copies, waits for them, and re-layouts: 1.64 us -> 4.8 us  [the longest x6 2.81 us: fused_shards(): jnp.transpose(signed, (0, 2, 1, 3, 5, 4))[:, :, :, :, :, None, :]]
    unnamed x7 -> x8, local copies, waits for them, and re-layouts: 5.67 us -> 3.57 us
where the time goes in v3:
time: 174 us
  Pallas kernels  155 us (89%)
  local copies, waits for them, and re-layouts  16.5 us (9%)
  other arithmetic  2.02 us (1%)
    pallas_call x1, Pallas kernels, fused_shards(): pl.pallas_call(functools.partial(fused_kernel, (layers, nd, nt, rows, mod...  155 us
    unnamed x8, local copies, waits for them, and re-layouts  3.57 us

profile of v3, /device:TPU:0, one launch (start us, length us, event | category | flops | bytes accessed | tf_op | source)
XLA Modules:
  0.0 173.9 jit_solution(18048396597921281513)
XLA Ops:
  0.7 0.7 tile.4
  1.5 0.6 broadcast_in_dim.4.lens
  2.1 0.8 reshape.77
  2.9 0.6 pad.16.skip
  3.5 1.4 reshape.76.gains
  4.9 0.9 add_divide_fusion
  6.0 0.6 pad_maximum_fusion.decay
  6.7 0.2 mul.140
  6.9 0.1 copy.22
  7.1 0.2 mul.134
  7.4 1.2 copy.19
  8.7 0.2 copy.21
  8.9 0.5 mul.137
  9.4 1.4 mul.138
  10.7 0.6 copy.23
  11.4 0.2 multiply_convert_fusion
  11.6 1.2 pad.15.outmix
  12.8 0.4 mul.131
  13.2 1.3 mul.132
  14.5 0.1 multiply_convert_fusion.1
  14.7 1.1 pad.14.inject
  15.7 154.6 %shard_map.158 = (bf16[256,512]{1,0:T(8,128)(2,1)}, f32[2,2,32,1024]{3,2,1,0:T(8,128)}) custom-call(bf16[256,512]{1,0:T(8,128)(2,1)} %bitcast.18, f32[8,128]{1,0:T(8,128)} %broadcast_in_dim.4.lens, f32[2,4,2,1,512]{4,3,2,1,0:T(1,128)} %reshape.76.gains, f32[2,2,4,1,256]{4,3,2,1,0:T(1,128)} %pad_maximum_fusion.decay, bf16[2,4,128,512]{3,2,1,0:T(8,128)(2,1)} %pad.14.inject, ...), custom_call_target="tpu_custom_call" | custom-call | tf_op jit(solution)/shard_map/pallas_call | solution.py:613
  170.4 1.7 copy.26
  172.0 1.9 %copy.27 = f32[2,2,32,1024]{3,2,1,0:T(8,128)} copy(f32[2,2,32,1024]{3,2,1,0:T(8,128)} %get-tuple-element.17) | data formatting | bytes 1048576
  (18 shorter events, 0.8 us)
Async XLA Ops:
  0.6 6.6 %copy-start.1 = (f32[2,2,16,64,16]{3,4,2,1,0:T(8,128)S(1)}, f32[2,2,16,64,16]{3,4,2,1,0:T(8,128)}, u32[]{:S(2)}) copy-start(f32[2,2,16,64,16]{3,4,2,1,0:T(8,128)} %param.26) | copy-start | bytes 786436
  6.9 1.8 %copy-start.2 = (f32[2,2,16,16,64]{4,3,2,1,0:T(8,128)S(1)}, f32[2,2,16,16,64]{4,3,2,1,0:T(8,128)}, u32[]{:S(2)}) copy-start(f32[2,2,16,16,64]{4,3,2,1,0:T(8,128)} %param.27) | copy-start | bytes 786436
  11.4 1.4 copy-start
